TPU v7x, 32 devices: a whole 2x2x4 slice. The times are simulated.
32 devices in a mesh: ep: 16 (over z, x, core), tp: 2 (over y).
Axes of the slice: x: 2, y: 2, z: 4, core: 2. Of those that a mesh axis runs over, the one named last changes fastest.
Arguments:
- mix_input: bfloat16 [8192, 1024], P(('ep', 'tp')), may hold values from -6 to 6
- pool_weight: bfloat16 [8, 128, 128], replicated, may hold values from -0.5 to 0.5
- pool_scale: float32 [1024], replicated, may hold values from 0.1 to 1.9
- out_weight: bfloat16 [1024, 2048], replicated, may hold values from -0.1875 to 0.1875
- moe_input: bfloat16 [2048, 2048], P('ep'), may hold values from -6 to 6
- moe_gain: float32 [2048], replicated, may hold values from 0.1 to 1.9
- group_router: bfloat16 [2048, 4], replicated, may hold values from -0.125 to 0.125
- inner_router: bfloat16 [2048, 16], replicated, may hold values from -0.125 to 0.125
- group_pick: int32 [2048], P('ep'), may hold values from 0 to 3
- inner_pick: int32 [2048, 2], P('ep'), may hold values from 0 to 3, all different within a row
- gate_weight: bfloat16 [16, 2048, 1024], P('ep', None, 'tp'), may hold values from -0.125 to 0.125
- up_weight: bfloat16 [16, 2048, 1024], P('ep', None, 'tp'), may hold values from -0.125 to 0.125
- down_weight: bfloat16 [16, 1024, 2048], P('ep', 'tp'), may hold values from -0.1875 to 0.1875
Outputs:
- mix_out: bfloat16 [8192, 2048], P(('ep', 'tp'))
- moe_out: bfloat16 [2048, 2048], P('ep', 'tp')
All inputs are finite; a program needn't handle non-finite values.
Results may differ from a plain program's by a relative error of at most 0.011.
Values may be sent and summed in bfloat16 or wider, within the bound.
No kernel may reach another device: no remote copies, remote signals or barrier semaphores. Data moves between devices by JAX's collectives and lax.ppermute only.
A program may use at most 64 MiB of HBM per device.

v0:
```python
import jax
import jax.numpy as jnp
from jax import lax
from jax.sharding import PartitionSpec as P

WINDOW_MAX = 16
NORM_FLOOR = 0.25


def passed_along(value, axis, steps):
    count = lax.axis_size(axis)
    first, last = (max(0, -steps), min(count, count - steps))
    return lax.ppermute(value, axis, [(source, source + steps) for source in range(first, last)])


def trailing_means(extended, row_count, lead_rows, first_position):
    group_width = extended.shape[1] // 4
    position = first_position + jnp.arange(row_count, dtype=jnp.int32)
    pieces = []
    for scale_index in range(4):
        window = 2 ** (scale_index + 1)
        channel_block = extended[:, scale_index * group_width : (scale_index + 1) * group_width]
        window_sum = channel_block[lead_rows : lead_rows + row_count]
        for back_step in range(1, window):
            window_sum = (
                window_sum
                + channel_block[lead_rows - back_step : lead_rows - back_step + row_count]
            )
        divisor = jnp.minimum(position + 1, window).astype(jnp.float32)
        pieces.append(window_sum / divisor[:, None])
    return jnp.concatenate(pieces, axis=1)


def route_terms(group_logits, inner_logits, group_pick, inner_pick, per_group):
    group_ids = jnp.arange(group_logits.shape[1], dtype=jnp.int32)
    chosen = jnp.sum(
        jnp.where(group_pick[:, None] == group_ids[None, :], group_logits, 0.0), axis=1
    )
    group_share = 1.0 / jnp.sum(jnp.exp(group_logits - chosen[:, None]), axis=1)
    target = group_pick[:, None] * per_group + inner_pick
    expert_ids = jnp.arange(inner_logits.shape[1], dtype=jnp.int32)
    picked = jnp.sum(
        jnp.where(target[:, :, None] == expert_ids[None, None, :], inner_logits[:, None, :], 0.0),
        axis=2,
    )
    first_share = jax.nn.sigmoid(picked[:, 0] - picked[:, 1])
    route_weight = group_share[:, None] * jnp.stack([first_share, 1.0 - first_share], axis=1)
    return (target, route_weight)


def slot_terms(target, expert_count, capacity):
    expert_ids = jnp.arange(expert_count, dtype=jnp.int32)
    expert_hits = (target[:, :, None] == expert_ids[None, None, :]).astype(jnp.int32)
    per_token = jnp.sum(expert_hits, axis=1)
    earlier = jnp.cumsum(per_token, axis=0) - per_token
    route_rank = jnp.sum(expert_hits * earlier[:, None, :], axis=2)
    is_kept = route_rank < capacity
    slot_index = target * capacity + jnp.minimum(route_rank, capacity - 1)
    return (slot_index, is_kept)


def slot_sources(slot_index, is_kept, slot_count):
    token_ids = jnp.broadcast_to(
        jnp.arange(slot_index.shape[0], dtype=jnp.int32)[:, None], slot_index.shape
    )
    placed = jnp.where(is_kept, slot_index, slot_count).reshape(-1)
    source = jnp.zeros((slot_count,), jnp.int32).at[placed].set(token_ids.reshape(-1), mode="drop")
    slot_used = jnp.zeros((slot_count,), jnp.bool_).at[placed].set(True, mode="drop")
    return (source, slot_used)


def per_device(
    mix_input,
    pool_weight,
    pool_scale,
    out_weight,
    moe_input,
    moe_gain,
    group_router,
    inner_router,
    group_pick,
    inner_pick,
    gate_weight,
    up_weight,
    down_weight,
):
    row_count = mix_input.shape[0]
    reach_back = WINDOW_MAX - 1
    before = passed_along(mix_input[row_count - reach_back :], ("ep", "tp"), 1)
    extended = jnp.concatenate([before, mix_input], axis=0).astype(jnp.float32)
    first_position = lax.axis_index(("ep", "tp")) * row_count
    trailing = (
        trailing_means(extended, row_count, reach_back, first_position) - extended[reach_back:]
    )
    pooled = trailing.astype(jnp.bfloat16)
    groups, group_dim = (pool_weight.shape[0], pool_weight.shape[1])
    grouped = jnp.einsum(
        "tgc,gcd->tgd",
        pooled.reshape(row_count, groups, group_dim),
        pool_weight,
        preferred_element_type=jnp.float32,
    )
    grouped = (grouped.reshape(row_count, groups * group_dim) * pool_scale[None, :]).astype(
        jnp.bfloat16
    )
    mix_out = jnp.dot(grouped, out_weight, preferred_element_type=jnp.float32).astype(jnp.bfloat16)
    tokens, feature_width = moe_input.shape
    token_values = moe_input.astype(jnp.float32)
    norm_scale = lax.rsqrt(
        jnp.maximum(jnp.mean(token_values * token_values, axis=1, keepdims=True), NORM_FLOOR)
    )
    normed = (token_values * norm_scale * moe_gain[None, :]).astype(jnp.bfloat16)
    group_logits = jnp.dot(normed, group_router, preferred_element_type=jnp.float32)
    inner_logits = jnp.dot(normed, inner_router, preferred_element_type=jnp.float32)
    group_count = group_router.shape[1]
    expert_count = inner_router.shape[1]
    target, route_weight = route_terms(
        group_logits, inner_logits, group_pick, inner_pick, expert_count // group_count
    )
    capacity = 2 * inner_pick.shape[1] * tokens // expert_count
    slot_index, is_kept = slot_terms(target, expert_count, capacity)
    source, slot_used = slot_sources(slot_index, is_kept, expert_count * capacity)
    gate_local = gate_weight[0]
    up_local = up_weight[0]
    outgoing = jnp.where(slot_used[:, None], normed[source], jnp.zeros((), jnp.bfloat16))
    arrived = lax.all_to_all(outgoing, "ep", split_axis=0, concat_axis=0, tiled=True)
    gate_sum = jnp.dot(arrived, gate_local, preferred_element_type=jnp.float32)
    up_sum = jnp.dot(arrived, up_local, preferred_element_type=jnp.float32)
    hidden = (jax.nn.silu(gate_sum) * up_sum).astype(jnp.bfloat16)
    down_local = down_weight[0]
    expert_result = lax.psum_scatter(
        lax.dot_general(
            down_local, hidden, (((0,), (1,)), ((), ())), preferred_element_type=jnp.float32
        ).astype(jnp.bfloat16),
        "tp",
        scatter_dimension=0,
        tiled=True,
    )
    returned = lax.all_to_all(expert_result, "ep", split_axis=1, concat_axis=1, tiled=True)
    route_scale = jnp.where(is_kept, route_weight, 0.0).astype(jnp.bfloat16)
    route_scale = lax.optimization_barrier(route_scale).astype(jnp.float32)
    picked = jnp.take(returned, slot_index, axis=1).astype(jnp.float32)
    combined = jnp.sum(picked * route_scale[None, :, :], axis=2)
    moe_out = combined.T.astype(jnp.bfloat16)
    return (mix_out, moe_out)


def solution(mesh):
    in_specs = (
        P(("ep", "tp"), None),
        P(),
        P(),
        P(),
        P("ep", None),
        P(),
        P(),
        P(),
        P("ep"),
        P("ep", None),
        P("ep", None, "tp"),
        P("ep", None, "tp"),
        P("ep", "tp", None),
    )
    out_specs = (P(("ep", "tp"), None), P("ep", "tp"))
    return jax.shard_map(
        per_device, mesh=mesh, in_specs=in_specs, out_specs=out_specs, check_vma=False
    )
```

profile of v0, /device:TPU:9, one launch (start us, length us, event | category | flops | bytes accessed | tf_op | source)
XLA Modules:
  0.0 159.9 jit_solution(5411471820745294769)
XLA Ops:
  7.2 0.0 copy-start
  7.2 0.0 reduce-scatter.2.cloned.1.call-start
  7.2 0.8 broadcast_multiply_fusion
  8.0 0.7 broadcast_add_fusion
  8.7 0.1 copy.31
  8.8 0.2 reduce_window_sum.11
  9.0 0.1 copy.33
  9.1 0.7 broadcast_select_fusion.2
  9.8 0.1 copy.35
  9.9 0.1 reshape.110
  10.1 0.1 reshape.140
  10.2 1.4 scatter_custom_fusion.1
  11.6 1.2 fusion.12
  12.9 1.5 scatter_custom_fusion
  14.4 0.1 broadcast_in_dim.88
  14.5 1.2 fusion.14
  15.7 3.3 %gather_fusion = bf16[512,2048]{1,0:T(8,128)(2,1)} fusion(bf16[128,2048]{1,0:T(8,128)(2,1)S(1)} %fusion.14, s32[1024]{0:T(1024)S(1)} %pad_clamp_fusion.1), kind=kCustom, calls=%fused_computation | custom fusion | bytes 4196352 | tf_op jit(solution)/shard_map/gather | solution.py:125
  19.1 1.8 %broadcast_select_fusion = bf16[16,32,2048]{2,1,0:T(8,128)(2,1)S(1)} fusion(bf16[16,32,2048]{2,1,0:T(8,128)(2,1)} %bitcast.45, pred[16,32]{1,0:T(8,128)(4,1)S(1)} %broadcast_in_dim.88), kind=kLoop, calls=%fused_computation.12 | loop fusion | flops 1048576 | bytes 4194816 | tf_op jit(solution)/shard_map/jit(_where)/select_n | solution.py:125
  20.9 0.0 copy-start.8
  20.9 54.3 %all_to_all.21 = bf16[16,32,2048]{2,1,0:T(8,128)(2,1)S(1)} all-to-all(bf16[16,32,2048]{2,1,0:T(8,128)(2,1)S(1)} %broadcast_select_fusion), channel_id=1, replica_groups=mesh['ep'=16,'tp'=2] {'ep'}, dimensions={0} | all-to-all | bytes 4194304 | tf_op jit(solution)/shard_map/all_to_all | solution.py:126
  75.2 0.0 copy-start.1
  75.2 1.3 copy-done.1
  76.5 0.0 copy-done.8
  76.5 2.2 %fusion.4 = f32[512,512]{1,0:T(8,128)} fusion(bf16[512,2048]{1,0:T(8,128)(2,1)S(1)} %bitcast.46, bf16[1,2048,512]{2,1,0:T(8,128)(2,1)S(1)} %copy-done.8), kind=kOutput, calls=%fused_computation.10 | convolution fusion | flops 1073741824 | bytes 5242880 | tf_op jit(solution)/shard_map/dot_general | solution.py:127
  78.7 0.0 copy-done
  78.7 6.3 %fusion = bf16[2048,512]{0,1:T(8,128)(2,1)} fusion(bf16[1,512,2048]{2,1,0:T(8,128)(2,1)S(1)} %copy-done, bf16[512,2048]{1,0:T(8,128)(2,1)} %bitcast.47, bf16[1,2048,512]{2,1,0:T(8,128)(2,1)} %param.24, f32[512,512]{1,0:T(8,128)} %fusion.4), kind=kOutput, calls=%fused_computation.5 | convolution fusion | flops 2150105088 | bytes 9437184 | tf_op jit(solution)/shard_map/dot_general | solution.py:132
  85.0 0.0 copy-start.3
  85.0 0.0 copy-start.6
  85.0 0.0 copy-start.2
  85.0 0.0 copy-start.4
  85.0 0.0 reduce-scatter.2.cloned.1.call-update
  85.0 0.8 slice.136
  85.8 3.1 %collective-permute-start = (bf16[15,1024]{1,0:T(8,128)(2,1)S(1)}, bf16[15,1024]{1,0:T(8,128)(2,1)S(1)}, u32[]{:S(2)}, u32[]{:S(2)}) collective-permute-start(bf16[15,1024]{1,0:T(8,128)(2,1)S(1)} %slice.136), channel_id=1, source_target_pairs={{0,1},{1,2},{2,3},{3,4},{4,5},{5,6},{6,7},{7,8},{8,9},{9,10},{10,1... | collective-permute-start | bytes 92168 | tf_op jit(solution)/shard_map/ppermute | solution.py:13
  89.0 0.0 copy-done.3
  89.0 0.0 copy-done.6
  89.0 0.3 select_reduce_fusion.2
  89.3 0.0 copy-done.2
  89.3 0.2 fusion.35
  89.6 0.0 copy-done.4
  89.6 26.4 %reduce-scatter.2.cloned.1.call-done = bf16[1024,512]{0,1:T(8,128)(2,1)} async-done(((bf16[2048,512]{0,1:T(8,128)(2,1)}), bf16[1024,512]{0,1:T(8,128)(2,1)}) %reduce-scatter.2.cloned.1.call-update) | async-done | bytes 1048592 | tf_op jit(solution)/shard_map/reduce_scatter | solution.py:131
  116.0 6.5 %all-to-all-start.1 = ((bf16[1024,16,32]{0,2,1:T(8,128)(2,1)}), bf16[1024,16,32]{0,2,1:T(8,128)(2,1)S(1)}, u32[]{:S(2)}, u32[]{:S(2)}) async-start(bf16[1024,16,32]{0,2,1:T(8,128)(2,1)} %bitcast.48), calls=%async_computation.2 | async-start | bytes 2097152 | tf_op jit(solution)/shard_map/all_to_all | solution.py:139
  122.6 0.1 copy.36
  122.7 0.1 reshape.122
  122.8 0.1 copy.37
  123.0 0.1 copy.34
  123.1 0.0 collective-permute-done
  123.1 1.2 maximum_convert_fusion
  124.3 0.3 fusion.24
  124.6 0.0 copy-start.9
  124.6 0.4 fusion.27
  125.0 0.6 copy-done.9
  125.6 0.0 copy-start.5
  125.6 0.0 copy-start.7
  125.6 0.3 fusion.19
  125.9 0.3 copy-done.5
  126.3 0.2 fusion.16
  126.5 1.3 copy-done.7
  127.8 2.2 %convolution_convert_fusion.1 = bf16[256,2048]{1,0:T(8,128)(2,1)} fusion(bf16[256,1024]{0,1:T(8,128)(2,1)S(1)} %fusion.16, bf16[1024,2048]{1,0:T(8,128)(2,1)S(1)} %copy-done.7), kind=kOutput, calls=%fused_computation.6 | convolution fusion | flops 1074266112 | bytes 5767168 | tf_op jit(solution)/shard_map/dot_general | solution.py:106
  130.0 17.4 %all-to-all-done.1 = bf16[1024,16,32]{0,2,1:T(8,128)(2,1)S(1)} async-done(((bf16[1024,16,32]{0,2,1:T(8,128)(2,1)}), bf16[1024,16,32]{0,2,1:T(8,128)(2,1)S(1)}, u32[]{:S(2)}, u32[]{:S(2)}) %all-to-all-start.1) | async-done | bytes 1048608 | tf_op jit(solution)/shard_map/all_to_all | solution.py:139
  147.5 2.0 %gather_fusion.1 = bf16[256,1024]{1,0:T(8,128)(2,1)} fusion(bf16[1024,512]{0,1:T(8,128)(2,1)S(1)} %bitcast.44, s32[1024]{0:T(1024)S(1)} %pad_clamp_fusion), kind=kCustom, calls=%fused_computation.1 | custom fusion | bytes 1049600 | tf_op jit(solution)/shard_map/jit(_take)/gather | solution.py:142
  149.4 1.2 reshape.125
  150.7 2.3 %multiply_reduce_fusion = bf16[128,1024]{1,0:T(8,128)(2,1)} fusion(bf16[128,2,1024]{2,1,0:T(2,128)(2,1)S(1)} %reshape.125, pred[128,2]{1,0:T(8,128)(4,1)S(1)} %copy.34, f32[128,2]{1,0:T(8,128)S(1)} %copy.37), kind=kLoop, calls=%fused_computation.24 | loop fusion | flops 917504 | bytes 787712 | tf_op jit(solution)/shard_map/reduce_sum | solution.py:143
  (18 shorter events, 0.2 us)
Async XLA Ops:
  7.2 71.5 %copy-start = (bf16[1,512,2048]{2,1,0:T(8,128)(2,1)S(1)}, bf16[1,512,2048]{2,1,0:T(8,128)(2,1)}, u32[]{:S(2)}) copy-start(bf16[1,512,2048]{2,1,0:T(8,128)(2,1)} %param.25) | copy-start | bytes 6291460
  7.2 108.8 %reduce-scatter.2.cloned.1.call-start = ((), (), s32[]{:S(2)}) async-start(), calls=%async_computation.3 | async-start | bytes 3145728 | tf_op jit(solution)/shard_map/reduce_scatter | solution.py:131
  20.9 55.6 %copy-start.8 = (bf16[1,2048,512]{2,1,0:T(8,128)(2,1)S(1)}, bf16[1,2048,512]{2,1,0:T(8,128)(2,1)}, u32[]{:S(2)}) copy-start(bf16[1,2048,512]{2,1,0:T(8,128)(2,1)} %param.23) | copy-start | bytes 6291460
  75.2 1.3 copy-start.1
  85.0 4.0 %copy-start.3 = (bf16[2048,4]{0,1:T(4,128)(2,1)S(1)}, bf16[2048,4]{0,1:T(4,128)(2,1)}, u32[]{:S(2)}) copy-start(bf16[2048,4]{0,1:T(4,128)(2,1)} %param.19) | copy-start | bytes 49156
  85.0 4.0 %copy-start.6 = (s32[128]{0:T(128)S(1)}, s32[128]{0:T(128)}, u32[]{:S(2)}) copy-start(s32[128]{0:T(128)} %param.21) | copy-start | bytes 1540
  85.0 4.3 %copy-start.2 = (bf16[2048,16]{0,1:T(8,128)(2,1)S(1)}, bf16[2048,16]{0,1:T(8,128)(2,1)}, u32[]{:S(2)}) copy-start(bf16[2048,16]{0,1:T(8,128)(2,1)} %param.20) | copy-start | bytes 196612
  85.0 4.6 %copy-start.4 = (s32[128,2]{0,1:T(2,128)S(1)}, s32[128,2]{0,1:T(2,128)}, u32[]{:S(2)}) copy-start(s32[128,2]{0,1:T(2,128)} %param.22) | copy-start | bytes 3076
  85.8 37.3 %collective-permute-start = (bf16[15,1024]{1,0:T(8,128)(2,1)S(1)}, bf16[15,1024]{1,0:T(8,128)(2,1)S(1)}, u32[]{:S(2)}, u32[]{:S(2)}) collective-permute-start(bf16[15,1024]{1,0:T(8,128)(2,1)S(1)} %slice.136), channel_id=1, source_target_pairs={{0,1},{1,2},{2,3},{3,4},{4,5},{5,6},{6,7},{7,8},{8,9},{9,10},{10,1... | collective-permute-start | bytes 92168 | tf_op jit(solution)/shard_map/ppermute | solution.py:13
  116.0 31.4 %all-to-all-start.1 = ((bf16[1024,16,32]{0,2,1:T(8,128)(2,1)}), bf16[1024,16,32]{0,2,1:T(8,128)(2,1)S(1)}, u32[]{:S(2)}, u32[]{:S(2)}) async-start(bf16[1024,16,32]{0,2,1:T(8,128)(2,1)} %bitcast.48), calls=%async_computation.2 | async-start | bytes 2097152 | tf_op jit(solution)/shard_map/all_to_all | solution.py:139
  124.6 1.0 copy-start.9
  125.6 0.7 copy-start.5
  125.6 2.2 %copy-start.7 = (bf16[1024,2048]{1,0:T(8,128)(2,1)S(1)}, bf16[1024,2048]{1,0:T(8,128)(2,1)}, u32[]{:S(2)}) copy-start(bf16[1024,2048]{1,0:T(8,128)(2,1)} %param.16) | copy-start | bytes 12582916
Sparse Core Ops, SparseCore 0:
  85.1 30.8 reduce-scatter.1
where the time goes:
time: 160 us
  blocking collectives  54.3 us (34%)
  waiting for transfers between devices  43.8 us (27%)
  local copies, waits for them, and re-layouts  14.9 us (9%)
  between operations  14.3 us (9%)
  matrix products  11.6 us (7%)
  other arithmetic  11.2 us (7%)
  starting transfers between devices  9.71 us (6%)
    all_to_all x1, blocking collectives, per_device(): lax.all_to_all(outgoing, 'ep', split_axis=0, concat_axis=0, tiled=True)  54.3 us
    reduce_scatter x1, waiting for transfers between devices, per_device(): lax.psum_scatter(lax.dot_general(down_local, hidden, (((0,), (1,)), ((),...  26.4 us
    all_to_all x1, waiting for transfers between devices, per_device(): lax.all_to_all(expert_result, 'ep', split_axis=1, concat_axis=1, tiled=True)  17.4 us
    all_to_all x1, starting transfers between devices, per_device(): lax.all_to_all(expert_result, 'ep', split_axis=1, concat_axis=1, tiled=True)  6.52 us
    dot_general x1, matrix products, per_device(): lax.dot_general(down_local, hidden, (((0,), (1,)), ((), ())), preferred_e...  6.27 us
    unnamed x20, local copies, waits for them, and re-layouts  3.54 us
    gather x1, local copies, waits for them, and re-layouts, per_device(): normed[source]  3.35 us
  transfers between devices with their start and end apart: 3, of which 2 were waited for; matrix products, arithmetic and copies ran while one was open for 4% of the time, Pallas kernels for 0%

commit v1 on v0

--- a/solution.py
+++ b/solution.py
@@ -2,6 +2,7 @@
 import jax.numpy as jnp
 from jax import lax
 from jax.sharding import PartitionSpec as P
+from jax.lax import all_to_all, axis_size
 
 WINDOW_MAX = 16
 NORM_FLOOR = 0.25
@@ -136,7 +137,9 @@
         scatter_dimension=0,
         tiled=True,
     )
-    returned = lax.all_to_all(expert_result, "ep", split_axis=1, concat_axis=1, tiled=True)
+    ready = axis_size("ep")
+    r1 = all_to_all(jnp.stack(jnp.split(expert_result, ready, axis=1)), "ep", 0, 0)
+    returned = jnp.concatenate(r1, axis=1)
     route_scale = jnp.where(is_kept, route_weight, 0.0).astype(jnp.bfloat16)
     route_scale = lax.optimization_barrier(route_scale).astype(jnp.float32)
     picked = jnp.take(returned, slot_index, axis=1).astype(jnp.float32)

time: 160 us -> 185 us (1.16)
  local copies, waits for them, and re-layouts: 14.9 us -> 38.3 us
    unnamed x20 -> x35, local copies, waits for them, and re-layouts: 3.54 us -> 25.5 us
  transfers between devices with their start and end apart: 3 -> 3, of which waited for: 2 -> 2; matrix products, arithmetic and copies ran while one was open for 4% -> 16% of each run, Pallas kernels for 0% -> 0%
where the time goes in v1:
time: 185 us; the launch traced here: 183 us
  blocking collectives  54.3 us (29%)
  waiting for transfers between devices  43.8 us (24%)
  local copies, waits for them, and re-layouts  38.3 us (21%)
  between operations  14.3 us (8%)
  matrix products  11.6 us (6%)
  other arithmetic  11.2 us (6%)
  starting transfers between devices  9.71 us (5%)
    all_to_all x1, blocking collectives, per_device(): lax.all_to_all(outgoing, 'ep', split_axis=0, concat_axis=0, tiled=True)  54.3 us
    reduce_scatter x1, waiting for transfers between devices, per_device(): lax.psum_scatter(lax.dot_general(down_local, hidden, (((0,), (1,)), ((),...  26.4 us
    unnamed x35, local copies, waits for them, and re-layouts  25.5 us
    all_to_all x1, waiting for transfers between devices, per_device(): all_to_all(jnp.stack(jnp.split(expert_result, ready, axis=1)), 'ep', 0, 0)  17.4 us
    all_to_all x1, starting transfers between devices, per_device(): all_to_all(jnp.stack(jnp.split(expert_result, ready, axis=1)), 'ep', 0, 0)  6.52 us
    dot_general x1, matrix products, per_device(): lax.dot_general(down_local, hidden, (((0,), (1,)), ((), ())), preferred_e...  6.27 us
  transfers between devices with their start and end apart: 3, of which 2 were waited for; matrix products, arithmetic and copies ran while one was open for 16% of the time, Pallas kernels for 0%

profile of v1, /device:TPU:9, one launch (start us, length us, event | category | flops | bytes accessed | tf_op | source)
XLA Modules:
  0.0 183.3 jit_solution(4304560074707034400)
XLA Ops:
  7.2 0.0 copy-start
  7.2 0.0 reduce-scatter.2.cloned.1.call-start
  7.2 0.8 broadcast_multiply_fusion
  8.0 0.7 broadcast_add_fusion
  8.7 0.1 copy.31
  8.8 0.2 reduce_window_sum.11
  9.0 0.1 copy.33
  9.1 0.7 broadcast_select_fusion.2
  9.8 0.1 copy.35
  9.9 0.1 reshape.114
  10.1 0.1 reshape.146
  10.2 1.4 scatter_custom_fusion.1
  11.6 1.2 fusion.12
  12.9 1.5 scatter_custom_fusion
  14.4 0.1 broadcast_in_dim.88
  14.5 1.2 fusion.14
  15.7 3.3 %gather_fusion = bf16[512,2048]{1,0:T(8,128)(2,1)} fusion(bf16[128,2048]{1,0:T(8,128)(2,1)S(1)} %fusion.14, s32[1024]{0:T(1024)S(1)} %pad_clamp_fusion.1), kind=kCustom, calls=%fused_computation | custom fusion | bytes 4196352 | tf_op jit(solution)/shard_map/gather | solution.py:126
  19.1 1.8 broadcast_select_fusion
  20.9 0.0 copy-start.8
  20.9 54.3 %all_to_all.14 = bf16[16,32,2048]{2,1,0:T(8,128)(2,1)S(1)} all-to-all(bf16[16,32,2048]{2,1,0:T(8,128)(2,1)S(1)} %broadcast_select_fusion), channel_id=1, replica_groups=mesh['ep'=16,'tp'=2] {'ep'}, dimensions={0} | all-to-all | bytes 4194304 | tf_op jit(solution)/shard_map/all_to_all | solution.py:127
  75.2 1.3 copy-done.1
  76.5 2.2 %fusion.4 = f32[512,512]{1,0:T(8,128)} fusion(bf16[512,2048]{1,0:T(8,128)(2,1)S(1)} %bitcast.111, bf16[1,2048,512]{2,1,0:T(8,128)(2,1)S(1)} %copy-done.8), kind=kOutput, calls=%fused_computation.10 | convolution fusion | flops 1073741824 | bytes 5242880 | tf_op jit(solution)/shard_map/dot_general | solution.py:128
  78.7 6.3 %fusion = bf16[2048,512]{0,1:T(8,128)(2,1)} fusion(bf16[1,512,2048]{2,1,0:T(8,128)(2,1)S(1)} %copy-done, bf16[512,2048]{1,0:T(8,128)(2,1)} %bitcast.112, bf16[1,2048,512]{2,1,0:T(8,128)(2,1)} %param.24, f32[512,512]{1,0:T(8,128)} %fusion.4), kind=kOutput, calls=%fused_computation.5 | convolution fusion | flops 2150105088 | bytes 9437184 | tf_op jit(solution)/shard_map/dot_general | solution.py:133
  85.0 0.0 reduce-scatter.2.cloned.1.call-update
  85.0 0.8 slice.136
  85.8 3.1 %collective-permute-start = (bf16[15,1024]{1,0:T(8,128)(2,1)S(1)}, bf16[15,1024]{1,0:T(8,128)(2,1)S(1)}, u32[]{:S(2)}, u32[]{:S(2)}) collective-permute-start(bf16[15,1024]{1,0:T(8,128)(2,1)S(1)} %slice.136), channel_id=1, source_target_pairs={{0,1},{1,2},{2,3},{3,4},{4,5},{5,6},{6,7},{7,8},{8,9},{9,10},{10,1... | collective-permute-start | bytes 92168 | tf_op jit(solution)/shard_map/ppermute | solution.py:14
  89.0 0.3 select_reduce_fusion.2
  89.3 0.2 fusion.51
  89.6 26.4 %reduce-scatter.2.cloned.1.call-done = bf16[1024,512]{0,1:T(8,128)(2,1)} async-done(((bf16[2048,512]{0,1:T(8,128)(2,1)}), bf16[1024,512]{0,1:T(8,128)(2,1)}) %reduce-scatter.2.cloned.1.call-update) | async-done | bytes 1048592 | tf_op jit(solution)/shard_map/reduce_scatter | solution.py:132
  116.0 1.5 fusion.43
  117.5 1.5 fusion.42
  118.9 1.5 fusion.41
  120.4 1.5 fusion.40
  121.9 1.5 fusion.39
  123.3 1.5 fusion.38
  124.8 1.5 fusion.37
  126.3 1.5 fusion.36
  127.7 1.5 fusion.35
  129.2 1.5 fusion.34
  130.6 1.5 fusion.33
  132.1 1.5 fusion.32
  133.6 1.5 fusion.31
  135.0 1.5 fusion.30
  136.5 1.5 fusion.29
  137.9 1.5 fusion.28
  139.4 6.5 %all-to-all-start.1 = ((bf16[16,1024,32]{1,2,0:T(8,128)(2,1)}), bf16[16,1024,32]{1,2,0:T(8,128)(2,1)S(1)}, u32[]{:S(2)}, u32[]{:S(2)}) async-start(bf16[16,1024,32]{1,2,0:T(8,128)(2,1)} %fusion.28), calls=%async_computation.2 | async-start | bytes 2097152 | tf_op jit(solution)/shard_map/all_to_all | solution.py:141
  146.0 0.1 copy.36
  146.1 0.1 reshape.128
  146.2 0.1 copy.37
  146.4 0.1 copy.34
  146.5 1.2 maximum_convert_fusion
  147.7 0.3 fusion.24
  148.0 0.0 copy-start.9
  148.0 0.4 fusion.27
  148.4 0.6 copy-done.9
  149.0 0.3 fusion.19
  149.3 0.3 copy-done.5
  149.7 0.2 fusion.16
  149.9 1.3 copy-done.7
  151.2 2.2 %convolution_convert_fusion.1 = bf16[256,2048]{1,0:T(8,128)(2,1)} fusion(bf16[256,1024]{0,1:T(8,128)(2,1)S(1)} %fusion.16, bf16[1024,2048]{1,0:T(8,128)(2,1)S(1)} %copy-done.7), kind=kOutput, calls=%fused_computation.6 | convolution fusion | flops 1074266112 | bytes 5767168 | tf_op jit(solution)/shard_map/dot_general | solution.py:107
  153.4 17.4 %all-to-all-done.1 = bf16[16,1024,32]{1,2,0:T(8,128)(2,1)S(1)} async-done(((bf16[16,1024,32]{1,2,0:T(8,128)(2,1)}), bf16[16,1024,32]{1,2,0:T(8,128)(2,1)S(1)}, u32[]{:S(2)}, u32[]{:S(2)}) %all-to-all-start.1) | async-done | bytes 1048608 | tf_op jit(solution)/shard_map/all_to_all | solution.py:141
  170.9 2.0 %gather_fusion.1 = bf16[256,1024]{1,0:T(8,128)(2,1)} fusion(bf16[1024,512]{0,1:T(8,128)(2,1)S(1)} %bitcast.109, s32[1024]{0:T(1024)S(1)} %pad_clamp_fusion), kind=kCustom, calls=%fused_computation.1 | custom fusion | bytes 1049600 | tf_op jit(solution)/shard_map/jit(_take)/gather | solution.py:145
  172.8 1.2 reshape.131
  174.1 2.3 %multiply_reduce_fusion = bf16[128,1024]{1,0:T(8,128)(2,1)} fusion(bf16[128,2,1024]{2,1,0:T(2,128)(2,1)S(1)} %reshape.131, pred[128,2]{1,0:T(8,128)(4,1)S(1)} %copy.34, f32[128,2]{1,0:T(8,128)S(1)} %copy.37), kind=kLoop, calls=%fused_computation.24 | loop fusion | flops 917504 | bytes 787712 | tf_op jit(solution)/shard_map/reduce_sum | solution.py:146
  (32 shorter events, 0.2 us)
Async XLA Ops:
  7.2 71.5 %copy-start = (bf16[1,512,2048]{2,1,0:T(8,128)(2,1)S(1)}, bf16[1,512,2048]{2,1,0:T(8,128)(2,1)}, u32[]{:S(2)}) copy-start(bf16[1,512,2048]{2,1,0:T(8,128)(2,1)} %param.25) | copy-start | bytes 6291460
  7.2 108.8 %reduce-scatter.2.cloned.1.call-start = ((), (), s32[]{:S(2)}) async-start(), calls=%async_computation.3 | async-start | bytes 3145728 | tf_op jit(solution)/shard_map/reduce_scatter | solution.py:132
  20.9 55.6 %copy-start.8 = (bf16[1,2048,512]{2,1,0:T(8,128)(2,1)S(1)}, bf16[1,2048,512]{2,1,0:T(8,128)(2,1)}, u32[]{:S(2)}) copy-start(bf16[1,2048,512]{2,1,0:T(8,128)(2,1)} %param.23) | copy-start | bytes 6291460
  75.2 1.3 copy-start.1
  85.0 4.0 %copy-start.3 = (bf16[2048,4]{0,1:T(4,128)(2,1)S(1)}, bf16[2048,4]{0,1:T(4,128)(2,1)}, u32[]{:S(2)}) copy-start(bf16[2048,4]{0,1:T(4,128)(2,1)} %param.19) | copy-start | bytes 49156
  85.0 4.0 %copy-start.6 = (s32[128]{0:T(128)S(1)}, s32[128]{0:T(128)}, u32[]{:S(2)}) copy-start(s32[128]{0:T(128)} %param.21) | copy-start | bytes 1540
  85.0 4.3 %copy-start.2 = (bf16[2048,16]{0,1:T(8,128)(2,1)S(1)}, bf16[2048,16]{0,1:T(8,128)(2,1)}, u32[]{:S(2)}) copy-start(bf16[2048,16]{0,1:T(8,128)(2,1)} %param.20) | copy-start | bytes 196612
  85.0 4.6 %copy-start.4 = (s32[128,2]{0,1:T(2,128)S(1)}, s32[128,2]{0,1:T(2,128)}, u32[]{:S(2)}) copy-start(s32[128,2]{0,1:T(2,128)} %param.22) | copy-start | bytes 3076
  85.8 60.7 %collective-permute-start = (bf16[15,1024]{1,0:T(8,128)(2,1)S(1)}, bf16[15,1024]{1,0:T(8,128)(2,1)S(1)}, u32[]{:S(2)}, u32[]{:S(2)}) collective-permute-start(bf16[15,1024]{1,0:T(8,128)(2,1)S(1)} %slice.136), channel_id=1, source_target_pairs={{0,1},{1,2},{2,3},{3,4},{4,5},{5,6},{6,7},{7,8},{8,9},{9,10},{10,1... | collective-permute-start | bytes 92168 | tf_op jit(solution)/shard_map/ppermute | solution.py:14
  139.4 31.4 %all-to-all-start.1 = ((bf16[16,1024,32]{1,2,0:T(8,128)(2,1)}), bf16[16,1024,32]{1,2,0:T(8,128)(2,1)S(1)}, u32[]{:S(2)}, u32[]{:S(2)}) async-start(bf16[16,1024,32]{1,2,0:T(8,128)(2,1)} %fusion.28), calls=%async_computation.2 | async-start | bytes 2097152 | tf_op jit(solution)/shard_map/all_to_all | solution.py:141
  148.0 1.0 copy-start.9
  149.0 0.7 copy-start.5
  149.0 2.2 %copy-start.7 = (bf16[1024,2048]{1,0:T(8,128)(2,1)S(1)}, bf16[1024,2048]{1,0:T(8,128)(2,1)}, u32[]{:S(2)}) copy-start(bf16[1024,2048]{1,0:T(8,128)(2,1)} %param.16) | copy-start | bytes 12582916
Sparse Core Ops, SparseCore 0:
  85.1 30.8 reduce-scatter.1
